TPU v7x, 32 devices: a whole 2x2x4 slice. The times are simulated.
32 devices in a mesh: ep: 4 (over y, x), tp: 8 (over z, core).
Axes of the slice: x: 2, y: 2, z: 4, core: 2. Of those that a mesh axis runs over, the one named last changes fastest.
Arguments:
- query_heads_rows: bfloat16 [2048, 2048], P('ep', 'tp'), may hold values from -9 to 9
- key_heads_rows: bfloat16 [2048, 2048], P('ep', 'tp'), may hold values from -9 to 9
- value_heads_rows: bfloat16 [2048, 2048], P('ep', 'tp'), may hold values from -6 to 6
- write_strength_logit: bfloat16 [16, 2048], P('tp', 'ep'), may hold values from -3.5 to -1
- decay_preactivation: bfloat16 [16, 2048], P('tp', 'ep'), may hold values from -5 to 5
- head_decay_logarithm: float32 [16], P('tp'), may hold values from -20 to -3
- extra_log_decay: float32 [16, 2048], P('tp', 'ep'), may hold values from -0.7 to 0
- output_weight: bfloat16 [2048, 2048], P('tp'), may hold values from -2 to 2
- second_batch_tokens: bfloat16 [4096, 2048], P(('ep', 'tp')), may hold values from -6 to 6
- expert_norm_scale: float32 [2048], replicated, may hold values from 0.1 to 1.9
- expert_choice_index: int32 [4096, 2], P(('ep', 'tp')), may hold values from 0 to 15, as said below
- group_router_weight: float32 [4096], P(('ep', 'tp')), may hold values from 0.25 to 1
- expert_logit_difference: float32 [4096], P(('ep', 'tp')), may hold values from -8 to 8
- expert_gate_weight: bfloat16 [16, 1024, 2048], P('ep', 'tp'), may hold values from -0.125 to 0.125
- expert_up_weight: bfloat16 [16, 1024, 2048], P('ep', 'tp'), may hold values from -0.125 to 0.125
- expert_down_weight: bfloat16 [16, 1024, 2048], P('ep', 'tp'), may hold values from -0.375 to 0.375
Outputs:
- mixer_output_first: bfloat16 [2048, 2048], P(('ep', 'tp'))
- expert_out: bfloat16 [4096, 2048], P(('ep', 'tp'))
Inputs may be any that keep to these rules, and one draw needn't show every extreme that they name: `expert_choice_index`: each row names two different experts of one group, the experts a * 4 to a * 4 + 3 for some a. In the rows of one device (aligned blocks of 128 rows) no expert is named more than 32 times, and in every device's rows some expert is named exactly 32 times.
All inputs are finite; a program needn't handle non-finite values.
Results may differ from a plain program's by a relative error of at most 0.018.
Values may be sent and summed in bfloat16 or wider, within the bound.
A program may use at most 128 MiB of HBM per device.

v0:
```python
import jax
import jax.numpy as jnp
from jax import lax
from jax.sharding import PartitionSpec as P

DK = 128
DV = 128
BLOCK = 64
CAP = 32
EXPERTS = 16
TOPK = 2
precise_setting = lax.Precision.HIGHEST
norm_eps = 1e-06


def prefix(value, axis, join, neutral):
    count, mine = (lax.axis_size(axis), lax.axis_index(axis))
    pieces = jax.tree.map(lambda part: lax.all_gather(part, axis), value)
    subtotal = jax.tree.map(
        lambda part, zero: jnp.full_like(part, 0) + jnp.asarray(zero, part.dtype), value, neutral
    )

    def step(position, subtotal):
        longer = join(subtotal, jax.tree.map(lambda part: part[position], pieces))
        return jax.tree.map(lambda new, old: jnp.where(position < mine, new, old), longer, subtotal)

    return lax.fori_loop(0, count - 1, step, subtotal)


def unit_rows(matrix):
    return matrix * lax.rsqrt(jnp.sum(matrix * matrix, axis=-1, keepdims=True) + norm_eps)


def block_terms(query_block, key_block, value_block, decay_logarithm, strength):
    span_len = query_block.shape[2]
    dim_value = value_block.shape[-1]
    cumulative = jnp.cumsum(decay_logarithm, axis=-1)
    within = jnp.tril(jnp.ones((span_len, span_len), bool))
    strict = jnp.tril(jnp.ones((span_len, span_len), bool), -1)
    spread = cumulative[..., :, None] - cumulative[..., None, :]
    decayed = jnp.where(within, jnp.exp(jnp.where(within, spread, 0.0)), 0.0)
    weighted = key_block * strength[..., None]
    lower_part = jnp.where(
        strict,
        jnp.einsum("hnid,hnjd->hnij", weighted, key_block, precision=precise_setting) * decayed,
        0.0,
    )
    system = lower_part + jnp.eye(span_len, dtype=jnp.float32)
    rhs_cols = jnp.concatenate(
        [value_block * strength[..., None], weighted * jnp.exp(cumulative)[..., None]], axis=-1
    )
    solved = jax.scipy.linalg.solve_triangular(system, rhs_cols, lower=True, unit_diagonal=True)
    updated_values = solved[..., :dim_value]
    delta_corrections = solved[..., dim_value:]
    scores = jnp.where(
        within,
        jnp.einsum("hnid,hnjd->hnij", query_block, key_block, precision=precise_setting) * decayed,
        0.0,
    )
    decayed_queries = query_block * jnp.exp(cumulative)[..., None]
    decayed_keys = key_block * jnp.exp(cumulative[..., -1:] - cumulative)[..., None]
    block_retention = jnp.exp(cumulative[..., -1])
    return (
        decayed_queries,
        decayed_keys,
        updated_values,
        delta_corrections,
        scores,
        block_retention,
    )


def carry_step(recurrent_state, inputs):
    decayed_queries, decayed_keys, updated_values, delta_corrections, scores, block_retention = (
        inputs
    )
    value_updates = updated_values - jnp.einsum(
        "jdb,jbu->jdu", delta_corrections, recurrent_state, precision=precise_setting
    )
    final_output = jnp.einsum(
        "jdb,jbu->jdu", decayed_queries, recurrent_state, precision=precise_setting
    )
    final_output = final_output + jnp.einsum(
        "hcj,hjv->hcv", scores, value_updates, precision=precise_setting
    )
    recurrent_state = recurrent_state * block_retention[:, None, None] + jnp.einsum(
        "rpq,rpd->rqd", decayed_keys, value_updates, precision=precise_setting
    )
    return (recurrent_state, final_output)


def compose(earlier, latter):
    joined_map = jnp.einsum("hij,hjk->hik", latter[0], earlier[0], precision=precise_setting)
    joined_state = (
        jnp.einsum("hij,hjv->hiv", latter[0], earlier[1], precision=precise_setting) + latter[1]
    )
    return (joined_map, joined_state)


def shards(
    query_heads_rows,
    key_heads_rows,
    value_heads_rows,
    write_strength_logit,
    decay_preactivation,
    head_decay_logarithm,
    extra_log_decay,
    output_weight,
    second_batch_tokens,
    expert_norm_scale,
    expert_choice_index,
    group_router_weight,
    expert_logit_difference,
    expert_gate_weight,
    expert_up_weight,
    expert_down_weight,
):
    length = query_heads_rows.shape[0]
    local_heads = head_decay_logarithm.shape[0]
    blocks = length // BLOCK
    width_model = output_weight.shape[1]

    def heads_first(matrix):
        spread_out = matrix.astype(jnp.float32).reshape(length, local_heads, -1).transpose(1, 0, 2)
        return spread_out.reshape(local_heads, blocks, BLOCK, -1)

    query_block = unit_rows(heads_first(query_heads_rows)) * DK ** (-0.5)
    key_block = unit_rows(heads_first(key_heads_rows))
    value_block = heads_first(value_heads_rows)
    strength = jax.nn.sigmoid(write_strength_logit.astype(jnp.float32)).reshape(
        local_heads, blocks, BLOCK
    )
    decay_logarithm = (
        -jnp.exp(head_decay_logarithm)[:, None]
        * jax.nn.softplus(decay_preactivation.astype(jnp.float32))
        + extra_log_decay
    )
    decay_logarithm = decay_logarithm.reshape(local_heads, blocks, BLOCK)
    decayed_queries, decayed_keys, updated_values, delta_corrections, scores, block_retention = (
        block_terms(query_block, key_block, value_block, decay_logarithm, strength)
    )
    fresh_wide = jnp.concatenate(
        [updated_values, jnp.zeros(updated_values.shape[:-1] + (DK,), jnp.float32)], axis=-1
    )
    inputs = tuple(
        (
            jnp.moveaxis(term, 1, 0)
            for term in (
                decayed_queries,
                decayed_keys,
                fresh_wide,
                delta_corrections,
                scores,
                block_retention,
            )
        )
    )
    identity_map = jnp.broadcast_to(jnp.eye(DK, dtype=jnp.float32), (local_heads, DK, DK))
    start_memory = jnp.concatenate(
        [jnp.zeros((local_heads, DK, DV), jnp.float32), identity_map], axis=-1
    )
    end_memory, outputs = lax.scan(carry_step, start_memory, inputs)
    local_output = outputs[..., :DV]
    projection_matrix = outputs[..., DV:]
    carried_end = end_memory[..., :DV]
    transfer = end_memory[..., DV:]
    _, incoming_rows = prefix(
        (transfer, carried_end), "ep", compose, (identity_map, jnp.zeros_like(carried_end))
    )
    attention_result = local_output + jnp.einsum(
        "xtyg,tgd->xtyd", projection_matrix, incoming_rows, precision=precise_setting
    )
    attn_rows = (
        attention_result.transpose(0, 2, 1, 3)
        .reshape(length, local_heads * DV)
        .astype(jnp.bfloat16)
    )
    summed = lax.psum_scatter(
        jnp.dot(attn_rows, output_weight, preferred_element_type=jnp.float32).astype(jnp.bfloat16),
        "tp",
        scatter_dimension=0,
        tiled=True,
    )
    widened = second_batch_tokens.astype(jnp.float32)
    normed = (
        widened
        * lax.rsqrt(jnp.mean(widened * widened, axis=-1, keepdims=True) + norm_eps)
        * expert_norm_scale
    ).astype(jnp.bfloat16)
    own_tokens = second_batch_tokens.shape[0]
    ep_count = lax.axis_size("ep")
    local_experts = EXPERTS // ep_count
    flat_ids = expert_choice_index.reshape(-1)
    one_hot = (flat_ids[:, None] == jnp.arange(EXPERTS, dtype=jnp.int32)[None, :]).astype(jnp.int32)
    slot_rank = jnp.sum((jnp.cumsum(one_hot, axis=0) - one_hot) * one_hot, axis=1)
    slot_index = flat_ids * CAP + slot_rank
    copy_token = jnp.arange(flat_ids.shape[0], dtype=jnp.int32) // TOPK
    slot_token = jnp.full((EXPERTS * CAP,), own_tokens, jnp.int32).at[slot_index].set(copy_token)
    outgoing = jnp.take(normed, slot_token, axis=0, mode="fill", fill_value=0).reshape(
        ep_count, local_experts, CAP, width_model
    )
    arrived = lax.all_to_all(outgoing, "ep", split_axis=0, concat_axis=0, tiled=True)
    gate_piece = lax.all_gather(expert_gate_weight, "tp", axis=1, tiled=True)
    up_piece = lax.all_gather(expert_up_weight, "tp", axis=1, tiled=True)
    down_piece = lax.all_gather(expert_down_weight, "tp", axis=1, tiled=True)
    gating = jnp.einsum("secd,efd->secf", arrived, gate_piece, preferred_element_type=jnp.float32)
    upward = jnp.einsum("secd,efd->secf", arrived, up_piece, preferred_element_type=jnp.float32)
    hidden = (jax.nn.silu(gating) * upward).astype(jnp.bfloat16)
    produced = jnp.einsum("secf,efd->secd", hidden, down_piece, preferred_element_type=jnp.float32)
    returned = lax.all_to_all(
        produced.astype(jnp.bfloat16), "ep", split_axis=0, concat_axis=0, tiled=True
    )
    flat_results = returned.reshape(EXPERTS * CAP, width_model)
    picked = (
        jnp.take(flat_results, slot_index, axis=0)
        .reshape(own_tokens, TOPK, width_model)
        .astype(jnp.float32)
    )
    leading = jax.nn.sigmoid(expert_logit_difference)
    mixing = group_router_weight[:, None] * jnp.stack([leading, 1.0 - leading], axis=-1)
    expert_out = jnp.sum(mixing[..., None] * picked, axis=1).astype(jnp.bfloat16)
    return (summed, expert_out)


def solution(mesh):
    in_specs = (
        P("ep", "tp"),
        P("ep", "tp"),
        P("ep", "tp"),
        P("tp", "ep"),
        P("tp", "ep"),
        P("tp"),
        P("tp", "ep"),
        P("tp", None),
        P(("ep", "tp"), None),
        P(),
        P(("ep", "tp"), None),
        P(("ep", "tp")),
        P(("ep", "tp")),
        P("ep", "tp", None),
        P("ep", "tp", None),
        P("ep", "tp", None),
    )
    out_specs = (P(("ep", "tp"), None), P(("ep", "tp"), None))
    return jax.shard_map(shards, mesh=mesh, in_specs=in_specs, out_specs=out_specs, check_vma=False)
```

profile of v0, /device:TPU:0, one launch (start us, length us, event | category | flops | bytes accessed | tf_op | source)
XLA Modules:
  0.0 520.2 jit_solution(1640668718798541853)
XLA Ops:
  13.5 3.3 gather_fusion
  16.9 3.1 broadcast_select_fusion
  20.0 5.6 %all-to-all-start = ((bf16[4,4,32,2048]{3,2,1,0:T(8,128)(2,1)}), bf16[4,4,32,2048]{3,2,1,0:T(8,128)(2,1)S(1)}, u32[]{:S(2)}, u32[]{:S(2)}) async-start(bf16[4,4,32,2048]{3,2,1,0:T(8,128)(2,1)} %broadcast_select_fusion), calls=%async_computation.1 | async-start | bytes 4194304 | tf_op jit(solution)/shard_map/all_to_all | solution.py:202
  29.5 3.0 fusion.52
  32.4 80.0 %custom-call.4 = f32[2,8,1,64,64]{3,4,2,1,0:T(8,128)} custom-call(f32[2,8,1,64,64]{4,3,2,1,0:T(8,128)} %fusion.52), custom_call_target="InvertDiagBlocksLowerTriangular" | custom-call | tf_op jit(solution)/shard_map/jit(_solve_triangular)/vmap(vmap())/triangular_solve | solution.py:52
  114.4 2.0 copy.100
  119.9 2.5 multiply_multiply_fusion
  125.6 2.0 fusion.50
  128.6 48.9 %while.26 = (s32[]{:T(128)}, f32[2,128,256]{2,1,0:T(8,128)S(1)}, f32[8,2,64,256]{3,2,0,1:T(8,128)}, f32[8,2]{1,0:T(8,128)}, f32[8,2,64,128]{3,2,0,1:T(8,128)}, /...) while((s32[]{:T(128)}, f32[2,128,256]{2,1,0:T(8,128)S(1)}, ...), condition=%wide.region_4.5_spmd, body=%wide.region_3.4_spmd.sunk | while | flops 176357376 | bytes 2231425 | solution.py:162
  173.8 1.8 fusion.127
  177.6 11.2 %all-gather = f32[8,128,128]{2,1,0:T(8,128)} all-gather(f32[2,128,128]{2,1,0:T(8,128)S(1)} %get-tuple-element.243), channel_id=2, replica_groups=mesh['ep'=4,'tp'=8] {'ep'}, dimensions={0}, use_global_device_ids=true | all-gather | bytes 655360 | tf_op jit(solution)/shard_map/all_gather | solution.py:18
  188.8 11.2 %all-gather.1 = f32[8,128,128]{2,1,0:T(8,128)} all-gather(f32[2,128,128]{2,1,0:T(8,128)S(1)} %get-tuple-element.242), channel_id=3, replica_groups=mesh['ep'=4,'tp'=8] {'ep'}, dimensions={0}, use_global_device_ids=true | all-gather | bytes 655360 | tf_op jit(solution)/shard_map/all_gather | solution.py:18
  200.1 4.0 while.27
  204.1 1.8 fusion.55
  206.2 2.1 convolution_convert_fusion
  208.4 12.9 %fusion.26 = f32[4,4,32,1024]{3,2,1,0:T(8,128)} fusion(bf16[4,1024,2048]{2,1,0:T(8,128)(2,1)} %all-gather.8.cloned.1.call-done, bf16[4,4,32,2048]{3,2,1,0:T(8,128)(2,1)S(1)} %all-to-all-done), kind=kOutput, calls=%fused_computation.34 | convolution fusion | flops 2147483648 | bytes 20971520 | tf_op jit(solution)/shard_map/secd,efd->secf/dot_general | solution.py:207
  221.3 93.1 %all-gather.6.cloned.1.call-done = bf16[4,1024,2048]{2,1,0:T(8,128)(2,1)} async-done(((bf16[4,128,2048]{2,1,0:T(8,128)(2,1)}), bf16[4,1024,2048]{2,1,0:T(8,128)(2,1)}) %all-gather.6.cloned.1.call-update) | async-done | bytes 16777232 | tf_op jit(solution)/shard_map/all_gather | solution.py:203
  314.3 13.1 %fusion.36 = bf16[4,4,32,1024]{3,2,0,1:T(8,128)(2,1)} fusion(f32[4,4,32,1024]{3,2,1,0:T(8,128)} %fusion.26, bf16[4,1024,2048]{2,1,0:T(8,128)(2,1)} %all-gather.6.cloned.1.call-done, bf16[4,4,32,2048]{3,2,1,0:T(8,128)(2,1)S(1)} %all-to-all-done), kind=kOutput, calls=%fused_computation.42 | convolution fusion | flops 2150629376 | bytes 22020096 | tf_op jit(solution)/shard_map/secd,efd->secf/dot_general | solution.py:206
  327.4 137.8 %all-gather.10.cloned.1.call-done = bf16[4,1024,2048]{2,1,0:T(8,128)(2,1)} async-done(((bf16[4,128,2048]{2,1,0:T(8,128)(2,1)}), bf16[4,1024,2048]{2,1,0:T(8,128)(2,1)}) %all-gather.10.cloned.1.call-update) | async-done | bytes 16777232 | tf_op jit(solution)/shard_map/all_gather | solution.py:205
  465.3 8.5 %fusion.33 = bf16[4,4,32,2048]{3,2,0,1:T(8,128)(2,1)S(1)} fusion(bf16[4,4,32,1024]{3,2,0,1:T(8,128)(2,1)} %fusion.36, bf16[4,1024,2048]{2,1,0:T(8,128)(2,1)} %all-gather.10.cloned.1.call-done), kind=kOutput, calls=%fused_computation.40 | convolution fusion | flops 2148532224 | bytes 19922944 | tf_op jit(solution)/shard_map/secf,efd->secd/dot_general | solution.py:209
  475.3 4.0 all-to-all-start.1
  479.9 24.7 %all-to-all-done.1 = bf16[4,4,32,2048]{3,2,1,0:T(8,128)(2,1)S(1)} async-done(((bf16[4,4,32,2048]{3,2,1,0:T(8,128)(2,1)}), bf16[4,4,32,2048]{3,2,1,0:T(8,128)(2,1)S(1)}, u32[]{:S(2)}, u32[]{:S(2)}) %all-to-all-start.1) | async-done | bytes 2097184 | tf_op jit(solution)/shard_map/all_to_all | solution.py:210
  504.6 2.3 gather_fusion.1
  508.7 4.9 multiply_reduce_fusion
  (172 shorter events, 74.4 us)
Async XLA Ops:
  7.2 199.1 %copy-start = (bf16[256,2048]{1,0:T(8,128)(2,1)S(1)}, bf16[256,2048]{1,0:T(8,128)(2,1)}, u32[]{:S(2)}) copy-start(bf16[256,2048]{1,0:T(8,128)(2,1)} %param.27) | copy-start | bytes 3145732
  7.2 201.2 %all-gather.8.cloned.1.call-start = ((), (), s32[]{:S(2)}) async-start(), calls=%async_computation.5 | async-start | bytes 18874368 | tf_op jit(solution)/shard_map/all_gather | solution.py:204
  7.9 5.2 %copy-start.2 = (bf16[128,2048]{1,0:T(8,128)(2,1)S(1)}, bf16[128,2048]{1,0:T(8,128)(2,1)}, u32[]{:S(2)}) copy-start(bf16[128,2048]{1,0:T(8,128)(2,1)} %param.28) | copy-start | bytes 1572868
  7.9 5.4 %copy-start.14 = (f32[2048]{0:T(1024)S(1)}, f32[2048]{0:T(1024)}, u32[]{:S(2)}) copy-start(f32[2048]{0:T(1024)} %param.29) | copy-start | bytes 24580
  7.9 306.4 %all-gather.6.cloned.1.call-start = ((), (), s32[]{:S(2)}) async-start(), calls=%async_computation.4 | async-start | bytes 18874368 | tf_op jit(solution)/shard_map/all_gather | solution.py:203
  8.7 456.6 %all-gather.10.cloned.1.call-start = ((), (), s32[]{:S(2)}) async-start(), calls=%async_computation.6 | async-start | bytes 18874368 | tf_op jit(solution)/shard_map/all_gather | solution.py:205
  20.0 5.6 %copy-start.23 = (f32[2]{0:T(128)S(1)}, f32[2]{0:T(128)}, u32[]{:S(2)}) copy-start(f32[2]{0:T(128)} %param.25) | copy-start | bytes 28
  20.0 5.6 %copy-start.19 = (f32[2,512]{1,0:T(2,128)S(1)}, f32[2,512]{1,0:T(2,128)}, u32[]{:S(2)}) copy-start(f32[2,512]{1,0:T(2,128)} %param.26) | copy-start | bytes 12292
  20.0 5.6 %copy-start.20 = (bf16[2,512]{1,0:T(2,128)(2,1)S(1)}, bf16[2,512]{1,0:T(2,128)(2,1)}, u32[]{:S(2)}) copy-start(bf16[2,512]{1,0:T(2,128)(2,1)} %param.24) | copy-start | bytes 6148
  20.0 5.8 %copy-start.6 = (bf16[512,256]{1,0:T(8,128)(2,1)S(1)}, bf16[512,256]{1,0:T(8,128)(2,1)}, u32[]{:S(2)}) copy-start(bf16[512,256]{1,0:T(8,128)(2,1)} %param.21) | copy-start | bytes 786436
  20.0 188.4 %all-to-all-start = ((bf16[4,4,32,2048]{3,2,1,0:T(8,128)(2,1)}), bf16[4,4,32,2048]{3,2,1,0:T(8,128)(2,1)S(1)}, u32[]{:S(2)}, u32[]{:S(2)}) async-start(bf16[4,4,32,2048]{3,2,1,0:T(8,128)(2,1)} %broadcast_select_fusion), calls=%async_computation.1 | async-start | bytes 4194304 | tf_op jit(solution)/shard_map/all_to_all | solution.py:202
  25.6 488.0 %reduce-scatter.2.cloned.1.call-start = ((), (), s32[]{:S(2)}) async-start(), calls=%async_computation.3 | async-start | bytes 2359296 | tf_op jit(solution)/shard_map/reduce_scatter | solution.py:178
  118.1 4.3 copy-start.7
  122.4 3.1 copy-start.5
  122.4 3.1 copy-start.8
  122.4 3.1 copy-start.16
  123.6 4.0 copy-start.21
  475.3 4.0 copy-start.10
  475.3 4.2 copy-start.12
  475.3 4.4 copy-start.24
  475.3 4.4 copy-start.22
  475.3 4.6 copy-start.18
  475.3 29.3 %all-to-all-start.1 = ((bf16[4,4,32,2048]{3,2,1,0:T(8,128)(2,1)}), bf16[4,4,32,2048]{3,2,1,0:T(8,128)(2,1)S(1)}, u32[]{:S(2)}, u32[]{:S(2)}) async-start(bf16[4,4,32,2048]{3,2,1,0:T(8,128)(2,1)} %copy.119), calls=%async_computation.2 | async-start | bytes 4194304 | tf_op jit(solution)/shard_map/all_to_all | solution.py:210
  504.6 9.0 %copy-start.1 = (bf16[256,2048]{1,0:T(8,128)(2,1)S(1)}, bf16[256,2048]{1,0:T(8,128)(2,1)}, u32[]{:S(2)}) copy-start(bf16[256,2048]{1,0:T(8,128)(2,1)} %param.27) | copy-start | bytes 3145732
  (7 other events, 7.6 us)
Sparse Core Ops, SparseCore 0:
  9.6 153.7 all-gather.7
  165.0 149.2 all-gather.5
  316.0 149.2 all-gather.9
  468.0 34.1 reduce-scatter.1
where the time goes:
time: 522 us; the launch traced here: 520 us
  waiting for transfers between devices  258 us (49%)
  other arithmetic  98.3 us (19%)
  matrix products  91.2 us (17%)
  local copies, waits for them, and re-layouts  26 us (5%)
  blocking collectives  22.5 us (4%)
  between operations  14.2 us (3%)
  starting transfers between devices  9.7 us (2%)
    all_gather x1, waiting for transfers between devices, shards(): down_piece = lax.all_gather(expert_down_weight, 'tp', axis=1, tiled=True)  138 us
    all_gather x1, waiting for transfers between devices, shards(): gate_piece = lax.all_gather(expert_gate_weight, 'tp', axis=1, tiled=True)  93.1 us
    another operation x2, other arithmetic, block_terms(): jax.scipy.linalg.solve_triangular(system, rhs_cols, lower=True, unit_diag...  80 us
    all_to_all x1, waiting for transfers between devices, shards(): lax.all_to_all(produced.astype(jnp.bfloat16), 'ep', split_axis=0, concat_...  24.7 us
    all_gather x2, blocking collectives, prefix(): pieces = jax.tree.map(lambda part: lax.all_gather(part, axis), value)  22.5 us
    dot_general x8, matrix products, carry_step(): jnp.einsum('hcj,hjv->hcv', scores, value_updates, precision=precise_setting)  14.2 us
    dot_general x1, matrix products, shards(): jnp.einsum('secd,efd->secf', arrived, gate_piece, preferred_element_type=...  13.1 us
    dot_general x1, matrix products, shards(): jnp.einsum('secd,efd->secf', arrived, up_piece, preferred_element_type=jn...  12.9 us
  transfers between devices with their start and end apart: 6, of which 3 were waited for; matrix products, arithmetic and copies ran while one was open for 41% of the time, Pallas kernels for 0%

commit v1 on v0

--- a/solution.py
+++ b/solution.py
@@ -200,10 +200,21 @@
         ep_count, local_experts, CAP, width_model
     )
     arrived = lax.all_to_all(outgoing, "ep", split_axis=0, concat_axis=0, tiled=True)
-    gate_piece = lax.all_gather(expert_gate_weight, "tp", axis=1, tiled=True)
     up_piece = lax.all_gather(expert_up_weight, "tp", axis=1, tiled=True)
     down_piece = lax.all_gather(expert_down_weight, "tp", axis=1, tiled=True)
-    gating = jnp.einsum("secd,efd->secf", arrived, gate_piece, preferred_element_type=jnp.float32)
+    peers, here, rows = (lax.axis_size("tp"), lax.axis_index("tp"), expert_gate_weight.shape[1])
+    ahead = [(i, (i + 1) % peers) for i in range(peers)]
+    held, out = (expert_gate_weight, None)
+    for hop in range(peers):
+        owner = (here - hop) % peers
+        upcoming = lax.ppermute(held, "tp", ahead) if hop < peers - 1 else None
+        made = jnp.einsum("secd,efd->secf", arrived, held, preferred_element_type=jnp.float32)
+        length_2 = made.shape[3]
+        if out is None:
+            out = jnp.zeros((*made.shape[:3], peers * length_2, *made.shape[3 + 1 :]), made.dtype)
+        out = lax.dynamic_update_slice_in_dim(out, made, owner * length_2, axis=3)
+        held = upcoming
+    gating = out
     upward = jnp.einsum("secd,efd->secf", arrived, up_piece, preferred_element_type=jnp.float32)
     hidden = (jax.nn.silu(gating) * upward).astype(jnp.bfloat16)
     produced = jnp.einsum("secf,efd->secd", hidden, down_piece, preferred_element_type=jnp.float32)

time: 522 us -> 580 us (1.11)
  the two profiles are of different devices: /device:TPU:0 before, /device:TPU:8 now
where the time goes in v1:
time: 580 us; the launch traced here: 578 us
  waiting for transfers between devices  185 us (32%)
  starting transfers between devices  164 us (28%)
  other arithmetic  92.6 us (16%)
  matrix products  86.4 us (15%)
  blocking collectives  21.7 us (4%)
  between operations  14.5 us (2%)
  local copies, waits for them, and re-layouts  13.4 us (2%)
    ppermute x7, waiting for transfers between devices, shards(): upcoming = lax.ppermute(held, 'tp', ahead) if hop < peers - 1 else None  160 us
    ppermute x7, starting transfers between devices, shards(): upcoming = lax.ppermute(held, 'tp', ahead) if hop < peers - 1 else None  155 us
    another operation x2, other arithmetic, block_terms(): jax.scipy.linalg.solve_triangular(system, rhs_cols, lower=True, unit_diag...  78.6 us
    all_to_all x1, waiting for transfers between devices, shards(): lax.all_to_all(produced.astype(jnp.bfloat16), 'ep', split_axis=0, concat_...  24.3 us
    dot_general x8, matrix products, shards(): jnp.einsum('secd,efd->secf', arrived, held, preferred_element_type=jnp.fl...  23 us
    all_gather x2, blocking collectives, prefix(): pieces = jax.tree.map(lambda part: lax.all_gather(part, axis), value)  21.7 us
    dot_general x8, matrix products, carry_step(): jnp.einsum('hcj,hjv->hcv', scores, value_updates, precision=precise_setting)  14.1 us
    dot_general x1, matrix products, shards(): jnp.einsum('secd,efd->secf', arrived, up_piece, preferred_element_type=jn...  12.2 us
  transfers between devices with their start and end apart: 12, of which 6 were waited for; matrix products, arithmetic and copies ran while one was open for 33% of the time, Pallas kernels for 0%

profile of v1, /device:TPU:8, one launch (start us, length us, event | category | flops | bytes accessed | tf_op | source)
XLA Modules:
  0.0 578.3 jit_solution(4147608489789610130)
XLA Ops:
  8.8 51.0 %collective-permute-done = bf16[4,128,2048]{2,1,0:T(8,128)(2,1)} collective-permute-done((bf16[4,128,2048]{2,1,0:T(8,128)(2,1)}, bf16[4,128,2048]{2,1,0:T(8,128)(2,1)}, u32[]{:S(2)}, u32[]{:S(2)}) %collective-permute-start) | collective-permute-done | bytes 2097184 | tf_op jit(solution)/shard_map/ppermute | solution.py:210
  59.8 20.9 %collective-permute-start.1 = (bf16[4,128,2048]{2,1,0:T(8,128)(2,1)}, bf16[4,128,2048]{2,1,0:T(8,128)(2,1)}, u32[]{:S(2)}, u32[]{:S(2)}) collective-permute-start(bf16[4,128,2048]{2,1,0:T(8,128)(2,1)} %collective-permute-done), channel_id=1, source_target_pairs={{0,1},{1,2},{2,3},{3,4},{4,5},{5,6},{6,7},{7,0},{8,9},{9,10},{10,1... | collective-permute-start | bytes 6291464 | tf_op jit(solution)/shard_map/ppermute | solution.py:210
  83.7 46.9 %collective-permute-done.1 = bf16[4,128,2048]{2,1,0:T(8,128)(2,1)} collective-permute-done((bf16[4,128,2048]{2,1,0:T(8,128)(2,1)}, bf16[4,128,2048]{2,1,0:T(8,128)(2,1)}, u32[]{:S(2)}, u32[]{:S(2)}) %collective-permute-start.1) | collective-permute-done | bytes 2097184 | tf_op jit(solution)/shard_map/ppermute | solution.py:210
  130.6 49.2 %collective-permute-start.2 = (bf16[4,128,2048]{2,1,0:T(8,128)(2,1)}, bf16[4,128,2048]{2,1,0:T(8,128)(2,1)}, u32[]{:S(2)}, u32[]{:S(2)}) collective-permute-start(bf16[4,128,2048]{2,1,0:T(8,128)(2,1)} %collective-permute-done.1), channel_id=1, source_target_pairs={{0,1},{1,2},{2,3},{3,4},{4,5},{5,6},{6,7},{7,0},{8,9},{9,10},{10,1... | collective-permute-start | bytes 6291464 | tf_op jit(solution)/shard_map/ppermute | solution.py:210
  180.3 3.3 gather_fusion
  183.7 3.1 broadcast_select_fusion
  186.8 4.6 all-to-all-start
  191.8 9.6 %collective-permute-done.2 = bf16[4,128,2048]{2,1,0:T(8,128)(2,1)} collective-permute-done((bf16[4,128,2048]{2,1,0:T(8,128)(2,1)}, bf16[4,128,2048]{2,1,0:T(8,128)(2,1)}, u32[]{:S(2)}, u32[]{:S(2)}) %collective-permute-start.2) | collective-permute-done | bytes 2097184 | tf_op jit(solution)/shard_map/ppermute | solution.py:210
  201.5 15.4 %collective-permute-start.3 = (bf16[4,128,2048]{2,1,0:T(8,128)(2,1)}, bf16[4,128,2048]{2,1,0:T(8,128)(2,1)}, u32[]{:S(2)}, u32[]{:S(2)}) collective-permute-start(bf16[4,128,2048]{2,1,0:T(8,128)(2,1)} %collective-permute-done.2), channel_id=1, source_target_pairs={{0,1},{1,2},{2,3},{3,4},{4,5},{5,6},{6,7},{7,0},{8,9},{9,10},{10,1... | collective-permute-start | bytes 6291464 | tf_op jit(solution)/shard_map/ppermute | solution.py:210
  219.4 24.5 %collective-permute-done.3 = bf16[4,128,2048]{2,1,0:T(8,128)(2,1)} collective-permute-done((bf16[4,128,2048]{2,1,0:T(8,128)(2,1)}, bf16[4,128,2048]{2,1,0:T(8,128)(2,1)}, u32[]{:S(2)}, u32[]{:S(2)}) %collective-permute-start.3) | collective-permute-done | bytes 2097184 | tf_op jit(solution)/shard_map/ppermute | solution.py:210
  243.9 35.0 %collective-permute-start.4 = (bf16[4,128,2048]{2,1,0:T(8,128)(2,1)}, bf16[4,128,2048]{2,1,0:T(8,128)(2,1)}, u32[]{:S(2)}, u32[]{:S(2)}) collective-permute-start(bf16[4,128,2048]{2,1,0:T(8,128)(2,1)} %collective-permute-done.3), channel_id=1, source_target_pairs={{0,1},{1,2},{2,3},{3,4},{4,5},{5,6},{6,7},{7,0},{8,9},{9,10},{10,1... | collective-permute-start | bytes 6291464 | tf_op jit(solution)/shard_map/ppermute | solution.py:210
  279.0 78.6 %custom-call.4 = f32[2,8,1,64,64]{3,4,2,1,0:T(8,128)S(1)} custom-call(f32[2,8,1,64,64]{4,3,2,1,0:T(8,128)S(1)} %fusion.59), custom_call_target="InvertDiagBlocksLowerTriangular" | custom-call | tf_op jit(solution)/shard_map/jit(_solve_triangular)/vmap(vmap())/triangular_solve | solution.py:52
  364.8 34.8 %collective-permute-start.5 = (bf16[4,128,2048]{2,1,0:T(8,128)(2,1)}, bf16[4,128,2048]{2,1,0:T(8,128)(2,1)}, u32[]{:S(2)}, u32[]{:S(2)}) collective-permute-start(bf16[4,128,2048]{2,1,0:T(8,128)(2,1)} %collective-permute-done.4), channel_id=1, source_target_pairs={{0,1},{1,2},{2,3},{3,4},{4,5},{5,6},{6,7},{7,0},{8,9},{9,10},{10,1... | collective-permute-start | bytes 6291464 | tf_op jit(solution)/shard_map/ppermute | solution.py:210
  399.6 35.7 %while.26 = (s32[]{:T(128)}, f32[2,128,256]{2,1,0:T(8,128)S(1)}, f32[8,2,64,256]{3,2,0,1:T(8,128)}, f32[8,2]{1,0:T(8,128)S(1)}, f32[8,2,64,128]{3,2,0,1:T(8,128)...) while((s32[]{:T(128)}, f32[2,128,256]{2,1,0:T(8,128)S(1)}, ...), condition=%wide.region_4.5_spmd, body=%wide.region_3.4_spmd.sunk | while | flops 176357376 | bytes 2231425 | solution.py:162
  435.3 10.9 %all-gather = f32[8,128,128]{2,1,0:T(8,128)S(1)} all-gather(f32[2,128,128]{2,1,0:T(8,128)S(1)} %get-tuple-element.243), channel_id=2, replica_groups=mesh['ep'=4,'tp'=8] {'ep'}, dimensions={0}, use_global_device_ids=true | all-gather | bytes 655360 | tf_op jit(solution)/shard_map/all_gather | solution.py:18
  446.2 10.8 %all-gather.1 = f32[8,128,128]{2,1,0:T(8,128)S(1)} all-gather(f32[2,128,128]{2,1,0:T(8,128)S(1)} %get-tuple-element.242), channel_id=3, replica_groups=mesh['ep'=4,'tp'=8] {'ep'}, dimensions={0}, use_global_device_ids=true | all-gather | bytes 655360 | tf_op jit(solution)/shard_map/all_gather | solution.py:18
  473.3 3.0 fusion.90
  476.2 3.0 fusion.96
  482.2 27.5 %collective-permute-done.6 = bf16[4,128,2048]{2,1,0:T(8,128)(2,1)S(1)} collective-permute-done((bf16[4,128,2048]{2,1,0:T(8,128)(2,1)}, bf16[4,128,2048]{2,1,0:T(8,128)(2,1)S(1)}, u32[]{:S(2)}, u32[]{:S(2)}) %collective-permute-start.6) | collective-permute-done | bytes 2097184 | tf_op jit(solution)/shard_map/ppermute | solution.py:210
  512.0 12.2 %fusion.50 = bf16[4,4,32,1024]{3,2,0,1:T(8,128)(2,1)S(1)} fusion(f32[4,4,32,1024]{3,2,0,1:T(8,128)S(1)} %fusion.108, bf16[4,1024,2048]{2,1,0:T(8,128)(2,1)} %all-gather.5.cloned.1.call-done, bf16[4,4,32,2048]{3,2,1,0:T(8,128)(2,1)} %all-to-all-done), kind=kOutput, calls=%fused_computation.56 | convolution fusion | flops 2150629376 | bytes 22020096 | tf_op jit(solution)/shard_map/secd,efd->secf/dot_general | solution.py:218
  524.2 8.1 %fusion.31 = bf16[4,4,32,2048]{3,2,0,1:T(8,128)(2,1)S(1)} fusion(bf16[4,4,32,1024]{3,2,0,1:T(8,128)(2,1)S(1)} %fusion.50, bf16[4,1024,2048]{2,1,0:T(8,128)(2,1)} %all-gather.7.cloned.1.call-done), kind=kOutput, calls=%fused_computation.38 | convolution fusion | flops 2148532224 | bytes 19922944 | tf_op jit(solution)/shard_map/secf,efd->secd/dot_general | solution.py:220
  534.0 4.0 all-to-all-start.1
  538.5 24.3 %all-to-all-done.1 = bf16[4,4,32,2048]{3,2,1,0:T(8,128)(2,1)S(1)} async-done(((bf16[4,4,32,2048]{3,2,1,0:T(8,128)(2,1)}), bf16[4,4,32,2048]{3,2,1,0:T(8,128)(2,1)S(1)}, u32[]{:S(2)}, u32[]{:S(2)}) %all-to-all-start.1) | async-done | bytes 2097184 | tf_op jit(solution)/shard_map/all_to_all | solution.py:221
  566.9 4.9 multiply_reduce_fusion
  (171 shorter events, 78.8 us)
Async XLA Ops:
  7.2 451.7 %copy-start = (bf16[256,2048]{1,0:T(8,128)(2,1)S(1)}, bf16[256,2048]{1,0:T(8,128)(2,1)}, u32[]{:S(2)}) copy-start(bf16[256,2048]{1,0:T(8,128)(2,1)} %param.27) | copy-start | bytes 3145732
  7.2 73.5 %copy-start.6 = (s32[128,2]{0,1:T(2,128)S(1)}, s32[128,2]{0,1:T(2,128)}, u32[]{:S(2)}) copy-start(s32[128,2]{0,1:T(2,128)} %param.30) | copy-start | bytes 3076
  7.2 172.7 %copy-start.2 = (bf16[128,2048]{1,0:T(8,128)(2,1)S(1)}, bf16[128,2048]{1,0:T(8,128)(2,1)}, u32[]{:S(2)}) copy-start(bf16[128,2048]{1,0:T(8,128)(2,1)} %param.28) | copy-start | bytes 1572868
  7.2 172.9 %copy-start.7 = (f32[2048]{0:T(1024)S(1)}, f32[2048]{0:T(1024)}, u32[]{:S(2)}) copy-start(f32[2048]{0:T(1024)} %param.29) | copy-start | bytes 24580
  7.2 504.8 %all-gather.5.cloned.1.call-start = ((), (), s32[]{:S(2)}) async-start(), calls=%async_computation.4 | async-start | bytes 18874368 | tf_op jit(solution)/shard_map/all_gather | solution.py:203
  7.9 516.3 %all-gather.7.cloned.1.call-start = ((), (), s32[]{:S(2)}) async-start(), calls=%async_computation.5 | async-start | bytes 18874368 | tf_op jit(solution)/shard_map/all_gather | solution.py:204
  8.7 51.1 %collective-permute-start = (bf16[4,128,2048]{2,1,0:T(8,128)(2,1)}, bf16[4,128,2048]{2,1,0:T(8,128)(2,1)}, u32[]{:S(2)}, u32[]{:S(2)}) collective-permute-start(bf16[4,128,2048]{2,1,0:T(8,128)(2,1)} %param.33), channel_id=1, source_target_pairs={{0,1},{1,2},{2,3},{3,4},{4,5},{5,6},{6,7},{7,0},{8,9},{9,10},{10,1... | collective-permute-start | bytes 6291464 | tf_op jit(solution)/shard_map/ppermute | solution.py:210
  59.8 70.8 %collective-permute-start.1 = (bf16[4,128,2048]{2,1,0:T(8,128)(2,1)}, bf16[4,128,2048]{2,1,0:T(8,128)(2,1)}, u32[]{:S(2)}, u32[]{:S(2)}) collective-permute-start(bf16[4,128,2048]{2,1,0:T(8,128)(2,1)} %collective-permute-done), channel_id=1, source_target_pairs={{0,1},{1,2},{2,3},{3,4},{4,5},{5,6},{6,7},{7,0},{8,9},{9,10},{10,1... | collective-permute-start | bytes 6291464 | tf_op jit(solution)/shard_map/ppermute | solution.py:210
  130.6 70.8 %collective-permute-start.2 = (bf16[4,128,2048]{2,1,0:T(8,128)(2,1)}, bf16[4,128,2048]{2,1,0:T(8,128)(2,1)}, u32[]{:S(2)}, u32[]{:S(2)}) collective-permute-start(bf16[4,128,2048]{2,1,0:T(8,128)(2,1)} %collective-permute-done.1), channel_id=1, source_target_pairs={{0,1},{1,2},{2,3},{3,4},{4,5},{5,6},{6,7},{7,0},{8,9},{9,10},{10,1... | collective-permute-start | bytes 6291464 | tf_op jit(solution)/shard_map/ppermute | solution.py:210
  186.8 4.7 copy-start.3
  186.8 4.9 copy-start.13
  186.8 4.9 copy-start.8
  186.8 5.0 copy-start.10
  186.8 30.2 %copy-start.9 = (bf16[2,512]{1,0:T(2,128)(2,1)S(1)}, bf16[2,512]{1,0:T(2,128)(2,1)}, u32[]{:S(2)}) copy-start(bf16[2,512]{1,0:T(2,128)(2,1)} %param.23) | copy-start | bytes 6148
  186.8 30.2 %copy-start.5 = (bf16[512,256]{1,0:T(8,128)(2,1)S(1)}, bf16[512,256]{1,0:T(8,128)(2,1)}, u32[]{:S(2)}) copy-start(bf16[512,256]{1,0:T(8,128)(2,1)} %param.20) | copy-start | bytes 786436
  186.8 274.3 %all-to-all-start = ((bf16[4,4,32,2048]{3,2,1,0:T(8,128)(2,1)}), bf16[4,4,32,2048]{3,2,1,0:T(8,128)(2,1)}, u32[]{:S(2)}, u32[]{:S(2)}) async-start(bf16[4,4,32,2048]{3,2,1,0:T(8,128)(2,1)} %broadcast_select_fusion), calls=%async_computation.1 | async-start | bytes 4194304 | tf_op jit(solution)/shard_map/all_to_all | solution.py:202
  191.4 380.3 %reduce-scatter.2.cloned.1.call-start = ((), (), s32[]{:S(2)}) async-start(), calls=%async_computation.3 | async-start | bytes 2359296 | tf_op jit(solution)/shard_map/reduce_scatter | solution.py:178
  201.5 42.5 %collective-permute-start.3 = (bf16[4,128,2048]{2,1,0:T(8,128)(2,1)}, bf16[4,128,2048]{2,1,0:T(8,128)(2,1)}, u32[]{:S(2)}, u32[]{:S(2)}) collective-permute-start(bf16[4,128,2048]{2,1,0:T(8,128)(2,1)} %collective-permute-done.2), channel_id=1, source_target_pairs={{0,1},{1,2},{2,3},{3,4},{4,5},{5,6},{6,7},{7,0},{8,9},{9,10},{10,1... | collective-permute-start | bytes 6291464 | tf_op jit(solution)/shard_map/ppermute | solution.py:210
  243.9 120.9 %collective-permute-start.4 = (bf16[4,128,2048]{2,1,0:T(8,128)(2,1)}, bf16[4,128,2048]{2,1,0:T(8,128)(2,1)}, u32[]{:S(2)}, u32[]{:S(2)}) collective-permute-start(bf16[4,128,2048]{2,1,0:T(8,128)(2,1)} %collective-permute-done.3), channel_id=1, source_target_pairs={{0,1},{1,2},{2,3},{3,4},{4,5},{5,6},{6,7},{7,0},{8,9},{9,10},{10,1... | collective-permute-start | bytes 6291464 | tf_op jit(solution)/shard_map/ppermute | solution.py:210
  364.8 99.5 %collective-permute-start.5 = (bf16[4,128,2048]{2,1,0:T(8,128)(2,1)}, bf16[4,128,2048]{2,1,0:T(8,128)(2,1)}, u32[]{:S(2)}, u32[]{:S(2)}) collective-permute-start(bf16[4,128,2048]{2,1,0:T(8,128)(2,1)} %collective-permute-done.4), channel_id=1, source_target_pairs={{0,1},{1,2},{2,3},{3,4},{4,5},{5,6},{6,7},{7,0},{8,9},{9,10},{10,1... | collective-permute-start | bytes 6291464 | tf_op jit(solution)/shard_map/ppermute | solution.py:210
  446.2 11.7 %copy-start.4 = (f32[8,2,64,256]{3,2,0,1:T(8,128)S(1)}, f32[8,2,64,256]{3,2,0,1:T(8,128)}, u32[]{:S(2)}) copy-start(f32[8,2,64,256]{3,2,0,1:T(8,128)} %get-tuple-element.144) | copy-start | bytes 3145732
  464.3 45.4 %collective-permute-start.6 = (bf16[4,128,2048]{2,1,0:T(8,128)(2,1)}, bf16[4,128,2048]{2,1,0:T(8,128)(2,1)S(1)}, u32[]{:S(2)}, u32[]{:S(2)}) collective-permute-start(bf16[4,128,2048]{2,1,0:T(8,128)(2,1)} %collective-permute-done.5), channel_id=1, source_target_pairs={{0,1},{1,2},{2,3},{3,4},{4,5},{5,6},{6,7},{7,0},{8,9},{9,10},{10,1... | collective-permute-start | bytes 6291464 | tf_op jit(solution)/shard_map/ppermute | solution.py:210
  534.0 28.8 %all-to-all-start.1 = ((bf16[4,4,32,2048]{3,2,1,0:T(8,128)(2,1)}), bf16[4,4,32,2048]{3,2,1,0:T(8,128)(2,1)S(1)}, u32[]{:S(2)}, u32[]{:S(2)}) async-start(bf16[4,4,32,2048]{3,2,1,0:T(8,128)(2,1)} %copy.133), calls=%async_computation.2 | async-start | bytes 4194304 | tf_op jit(solution)/shard_map/all_to_all | solution.py:221
  562.8 9.0 %copy-start.1 = (bf16[256,2048]{1,0:T(8,128)(2,1)S(1)}, bf16[256,2048]{1,0:T(8,128)(2,1)}, u32[]{:S(2)}) copy-start(bf16[256,2048]{1,0:T(8,128)(2,1)} %param.27) | copy-start | bytes 3145732
  (3 other events, 11.9 us)
Sparse Core Ops, SparseCore 0:
  9.6 211.4 all-gather.4
  222.7 191.9 all-gather.6
  461.1 36.5 reduce-scatter.1
